TPU v7x, 32 devices: a whole 2x2x4 slice. The times are simulated.
32 devices in a mesh: ep: 8 (over z, x), tp: 4 (over y, core).
Axes of the slice: x: 2, y: 2, z: 4, core: 2. Of those that a mesh axis runs over, the one named last changes fastest.
Arguments:
- memory_query_matrix: bfloat16 [4096, 1024], P('ep', 'tp'), may hold values from -0.59765625 to 2
- memory_key_matrix: bfloat16 [4096, 1024], P('ep', 'tp'), may hold values from -0.59765625 to 2
- memory_value_matrix: bfloat16 [4096, 1024], P('ep', 'tp'), may hold values from -6 to 6
- input_gate_logits: float32 [4, 4096], P('tp', 'ep'), may hold values from -6 to 260
- forget_gate_logits: float32 [4, 4096], P('tp', 'ep'), may hold values from -1 to 20
- forget_log_boosts: float32 [4, 4096], P('tp', 'ep'), may hold values from -0.7 to 0
- head_norm_scale: float32 [1024], P('tp'), may hold values from 0.1 to 1.9
- memory_output_matrix: bfloat16 [1024, 2048], replicated, may hold values from -0.1875 to 0.1875
- projection_norm_scale: float32 [2048], replicated, may hold values from 0.1 to 1.9
- second_batch_rows: bfloat16 [6144, 2048], P(('ep', 'tp')), may hold values from -6 to 6
- expert_prenorm_scale: float32 [2048], replicated, may hold values from 0.1 to 1.9
- selected_expert_index: int32 [6144, 2], P(('ep', 'tp')), may hold values from 0 to 7, all different within a row; in each aligned block of 192 rows (0 to 191, 192 to 383, ...) at most 96 rows name the same one
- group_route_probability: float32 [6144], P(('ep', 'tp')), may hold values from 0.2 to 1
- expert_choice_scores: float32 [6144, 2], P(('ep', 'tp')), may hold values from -6 to 6
- expert_gate_matrix: bfloat16 [8, 2048, 512], P('ep'), may hold values from -0.125 to 0.125
- expert_up_matrix: bfloat16 [8, 2048, 512], P('ep'), may hold values from -0.125 to 0.125
- expert_down_matrix: bfloat16 [8, 512, 2048], P('ep'), may hold values from -0.25 to 0.25
Outputs:
- mixed_rows: bfloat16 [4096, 2048], P(('ep', 'tp'))
- routed_rows: bfloat16 [6144, 2048], P(('ep', 'tp'))
Inputs may be any that keep to these rules, and one draw needn't show every extreme that they name: `selected_expert_index`: each row names 2 different experts; among the rows of one device no expert is named more than 96 times, and in some device one expert is named exactly that often.
All inputs are finite; a program needn't handle non-finite values.
Results may differ from a plain program's by a relative error of at most 0.013.
Values may be sent and summed in bfloat16 or wider, within the bound.
A program may use at most 128 MiB of HBM per device.

v0:
```python
import jax
import jax.numpy as jnp
from jax import lax
from jax.sharding import PartitionSpec as P

SPAN = 128


floor_log = -1e30
norm_eps = 1e-06
exact = lax.Precision.HIGHEST


def entering_2(array, axis, combine, identity):
    devices, position = (lax.axis_size(axis), lax.axis_index(axis))
    everything = jax.tree.map(lambda part: lax.all_gather(part, axis), array)
    start = jax.tree.map(
        lambda part, zero: jnp.broadcast_to(jnp.asarray(zero, part.dtype), part.shape),
        array,
        identity,
    )

    def step(k, before):
        reached = k < position
        new = combine(before, jax.tree.map(lambda part: part[k], everything))
        return jax.tree.map(lambda a, b: jnp.where(reached, a, b), new, before)

    return lax.fori_loop(0, devices, step, start)


def rms_scale(values, gain):
    squares = jnp.mean(values * values, axis=-1, keepdims=True)
    return values * lax.rsqrt(squares + norm_eps) * gain


def span_step(carry, inputs):
    memory, normer, stabil = carry
    query, keyrow, valrow, in_gate, log_retain_factor = inputs
    key_scale = query.shape[-1] ** (-0.5)
    length = query.shape[1]
    causal = jnp.tril(jnp.ones((length, length), dtype=bool))
    cumulative = jnp.cumsum(log_retain_factor, axis=-1)
    decay_map = cumulative[:, :, None] - cumulative[:, None, :] + in_gate[:, None, :]
    decay_map = jnp.where(causal[None], decay_map, -jnp.inf)
    carried = cumulative + stabil[:, None]
    peak = jnp.maximum(carried, jnp.max(decay_map, axis=-1))
    within = jnp.exp(decay_map - peak[:, :, None])
    across = jnp.exp(carried - peak)
    products = jnp.einsum("htd,hsd->hts", query, keyrow, preferred_element_type=jnp.float32)
    scores = products * key_scale * within
    qfloat = query.astype(jnp.float32)
    denominator = jnp.sum(scores, axis=-1) + across * jnp.einsum(
        "hd,htd->ht", normer, qfloat, precision=exact
    )
    weights = scores.astype(jnp.bfloat16)
    numerator = jnp.einsum("hts,hsd->htd", weights, valrow, preferred_element_type=jnp.float32)
    numerator = numerator + across[:, :, None] * jnp.einsum(
        "hed,htd->hte", memory, qfloat, precision=exact
    )
    output = numerator / jnp.maximum(jnp.abs(denominator), jnp.exp(-peak))[:, :, None]
    span_end = cumulative[:, -1]
    gap_log = span_end[:, None] - cumulative + in_gate
    new_peak = jnp.maximum(span_end + stabil, jnp.max(gap_log, axis=-1))
    shrink = jnp.exp(span_end + stabil - new_peak)
    spread = jnp.exp(gap_log - new_peak[:, None]) * key_scale
    keys_weighted = keyrow.astype(jnp.float32) * spread[:, :, None]
    memory = shrink[:, None, None] * memory + jnp.einsum(
        "hse,hsd->hed", valrow.astype(jnp.float32), keys_weighted, precision=exact
    )
    normer = shrink[:, None] * normer + jnp.sum(keys_weighted, axis=1)
    return ((memory, normer, new_peak), output)


def span_summary(keyrow, valrow, in_gate, log_retain_factor):
    key_scale = keyrow.shape[-1] ** (-0.5)
    cumulative = jnp.cumsum(log_retain_factor, axis=-1)
    span_end = cumulative[:, -1]
    gap_log = span_end[:, None] - cumulative + in_gate
    peak = jnp.max(gap_log, axis=-1)
    spread = jnp.exp(gap_log - peak[:, None]) * key_scale
    keys_weighted = keyrow.astype(jnp.float32) * spread[:, :, None]
    memory = jnp.einsum("hse,hsd->hed", valrow.astype(jnp.float32), keys_weighted, precision=exact)
    return (span_end, peak, memory, jnp.sum(keys_weighted, axis=1))


def join_states(earlier, later):
    total_early, peak_early, memory_early, normer_early = earlier
    total_late, peak_late, memory_late, normer_late = later
    peak = jnp.maximum(total_late + peak_early, peak_late)
    factor_early = jnp.exp(total_late + peak_early - peak)
    factor_late = jnp.exp(peak_late - peak)
    memory = factor_early[:, None, None] * memory_early + factor_late[:, None, None] * memory_late
    normer = factor_early[:, None] * normer_early + factor_late[:, None] * normer_late
    return (total_early + total_late, peak, memory, normer)


def shards(
    memory_query_matrix,
    memory_key_matrix,
    memory_value_matrix,
    input_gate_logits,
    forget_gate_logits,
    forget_log_boosts,
    head_norm_scale,
    memory_output_matrix,
    projection_norm_scale,
    second_batch_rows,
    expert_prenorm_scale,
    selected_expert_index,
    group_route_probability,
    expert_choice_scores,
    expert_gate_matrix,
    expert_up_matrix,
    expert_down_matrix,
):
    local_heads = input_gate_logits.shape[0]
    positions = input_gate_logits.shape[1]
    head_size = memory_query_matrix.shape[1] // local_heads
    spans = positions // SPAN

    def by_head(rows):
        return rows.reshape(positions, local_heads, head_size).transpose(1, 0, 2)

    def to_spans(values):
        shaped = values.reshape((local_heads, spans, SPAN) + values.shape[2:])
        return jnp.moveaxis(shaped, 1, 0)

    query = by_head(memory_query_matrix)
    keyrow = by_head(memory_key_matrix)
    valrow = by_head(memory_value_matrix)
    log_retain_factor = jax.nn.log_sigmoid(forget_gate_logits) + forget_log_boosts
    summary = span_summary(keyrow, valrow, input_gate_logits, log_retain_factor)
    neutral = (
        jnp.zeros((local_heads,), jnp.float32),
        jnp.full((local_heads,), floor_log, jnp.float32),
        jnp.zeros((local_heads, head_size, head_size), jnp.float32),
        jnp.zeros((local_heads, head_size), jnp.float32),
    )
    entering = entering_2(summary, "ep", join_states, neutral)
    start = (entering[2], entering[3], entering[1])
    inputs = (
        to_spans(query),
        to_spans(keyrow),
        to_spans(valrow),
        to_spans(input_gate_logits),
        to_spans(log_retain_factor),
    )
    _, cells = lax.scan(span_step, start, inputs)
    cells = jnp.moveaxis(cells, 0, 1).reshape(local_heads, positions, head_size)
    scaled = (cells * head_norm_scale.reshape(local_heads, 1, head_size)).astype(jnp.bfloat16)
    head_out = scaled.transpose(1, 0, 2).reshape(positions, local_heads * head_size)
    first_row = lax.axis_index("tp") * head_out.shape[1]
    weight_rows = lax.dynamic_slice_in_dim(memory_output_matrix, first_row, head_out.shape[1], 0)
    projected = lax.psum_scatter(
        jnp.dot(head_out, weight_rows, preferred_element_type=jnp.float32).astype(jnp.bfloat16),
        "tp",
        scatter_dimension=0,
        tiled=True,
    ).astype(jnp.float32)
    mixed_rows = rms_scale(projected, projection_norm_scale).astype(jnp.bfloat16)
    token_count = second_batch_rows.shape[0]
    choices_per = selected_expert_index.shape[1]
    experts = lax.axis_size("ep")
    capacity = 2 * choices_per * token_count // experts
    ffn_rows = rms_scale(second_batch_rows.astype(jnp.float32), expert_prenorm_scale).astype(
        jnp.bfloat16
    )
    flat_ids = selected_expert_index.reshape(-1)
    onehot = (flat_ids[:, None] == jnp.arange(experts, dtype=jnp.int32)[None, :]).astype(jnp.int32)
    rank = jnp.sum((jnp.cumsum(onehot, axis=0) - onehot) * onehot, axis=1)
    slot = flat_ids * capacity + rank
    placing = (jnp.arange(experts * capacity, dtype=jnp.int32)[:, None] == slot[None, :]).astype(
        jnp.bfloat16
    )
    placing = jnp.sum(placing.reshape(experts * capacity, token_count, choices_per), axis=-1)
    outgoing = jnp.dot(placing, ffn_rows, preferred_element_type=jnp.float32).astype(jnp.bfloat16)
    outgoing = outgoing.reshape(experts, capacity, ffn_rows.shape[1])
    w_gate = expert_gate_matrix[0]
    w_up = expert_up_matrix[0]
    w_down = expert_down_matrix[0]
    received = lax.all_to_all(outgoing, "ep", split_axis=0, concat_axis=0, tiled=True)
    flat_rows = received.reshape(-1, received.shape[2])
    gate = jnp.dot(flat_rows, w_gate, preferred_element_type=jnp.float32)
    upper = jnp.dot(flat_rows, w_up, preferred_element_type=jnp.float32)
    hidden = (jax.nn.silu(gate) * upper).astype(jnp.bfloat16)
    answer = jnp.dot(hidden, w_down, preferred_element_type=jnp.float32).astype(jnp.bfloat16)
    answers = answer.reshape(received.shape)
    back = lax.all_to_all(answers, "ep", split_axis=0, concat_axis=0, tiled=True)
    picked = back.reshape(experts * capacity, back.shape[2])[slot].reshape(
        token_count, choices_per, back.shape[2]
    )
    route_weight = group_route_probability[:, None] * jax.nn.softmax(expert_choice_scores, axis=-1)
    routed_rows = jnp.sum(route_weight[:, :, None] * picked.astype(jnp.float32), axis=1).astype(
        jnp.bfloat16
    )
    return (mixed_rows, routed_rows)


def solution(mesh):
    return jax.shard_map(
        shards,
        mesh=mesh,
        in_specs=(
            P("ep", "tp"),
            P("ep", "tp"),
            P("ep", "tp"),
            P("tp", "ep"),
            P("tp", "ep"),
            P("tp", "ep"),
            P("tp"),
            P(),
            P(),
            P(("ep", "tp"), None),
            P(),
            P(("ep", "tp"), None),
            P(("ep", "tp")),
            P(("ep", "tp"), None),
            P("ep", None, None),
            P("ep", None, None),
            P("ep", None, None),
        ),
        out_specs=(P(("ep", "tp"), None), P(("ep", "tp"), None)),
        check_vma=False,
    )
```

profile of v0, /device:TPU:0, one launch (start us, length us, event | category | flops | bytes accessed | tf_op | source)
XLA Modules:
  0.0 327.3 jit_solution(2145870936360990207)
XLA Ops:
  7.3 0.9 fusion.71
  8.9 0.7 slice.25
  9.6 2.0 fusion.76
  11.5 1.9 exponential_multiply_fusion.1
  13.5 2.4 convolution_bitcast_fusion.2
  15.9 0.8 copy.34
  17.0 0.9 reduce-window.16
  18.5 0.6 dynamic-slice
  19.1 1.3 bitcast_dynamic-update-slice_fusion
  20.5 1.3 dynamic-update-slice.1
  22.2 2.8 convolution_convert_fusion.1
  25.0 7.4 %all-to-all-start = ((bf16[8,96,2048]{2,1,0:T(8,128)(2,1)}), bf16[8,96,2048]{2,1,0:T(8,128)(2,1)}, u32[]{:S(2)}, u32[]{:S(2)}) async-start(bf16[8,96,2048]{2,1,0:T(8,128)(2,1)} %bitcast.221), calls=%async_computation.1 | async-start | bytes 6291456 | tf_op jit(solution)/shard_map/all_to_all | solution.py:181
  32.5 86.9 %all-reduce.2 = (f32[8]{0:T(128)S(1)}, f32[8]{0:T(128)S(1)}) all-reduce(f32[8]{0:T(128)S(1)} %bitcast_dynamic-update-slice_fusion, f32[8]{0:T(128)S(1)} %dynamic-update-slice.1), channel_id=1, replica_groups=mesh['ep'=8,'tp'=4] {'ep'}, use_global_device_ids=true, to_apply=%add | all-reduce | flops 16 | bytes 128
  119.5 32.2 %all-gather.2 = f32[8,1,256]{2,1,0:T(1,128)S(1)} all-gather(f32[1,1,256]{2,1,0:T(1,128)S(1)} %bitcast.240), channel_id=3, replica_groups=mesh['ep'=8,'tp'=4] {'ep'}, dimensions={0}, use_global_device_ids=true | all-gather | bytes 9216 | tf_op jit(solution)/shard_map/all_gather | solution.py:16
  151.7 2.9 copy.38
  154.6 29.8 %while.35 = (s32[]{:T(128)}, f32[1]{0:T(128)}, f32[1,256,256]{2,1,0:T(8,128)S(1)}, f32[1,256]{1,0:T(1,128)S(1)}, s32[]{:T(128)}, /*index=5*/f32[8,1]{0,1:T(1,128...) while((s32[]{:T(128)}, f32[1]{0:T(128)}, ...), condition=%wide.region_5.6_spmd.clone, body=%wide.region_4.5_spmd.clone.sunk | while | flops 328969 | bytes 789756 | solution.py:28
  157.2 1.1 fusion.121
  158.3 0.6 constant_dynamic-slice_fusion.5
  160.9 1.1 fusion.121
  162.1 0.6 constant_dynamic-slice_fusion.5
  164.6 1.1 fusion.121
  165.8 0.6 constant_dynamic-slice_fusion.5
  168.4 1.1 fusion.121
  169.5 0.6 constant_dynamic-slice_fusion.5
  172.1 1.1 fusion.121
  173.3 0.6 constant_dynamic-slice_fusion.5
  175.8 1.1 fusion.121
  177.0 0.6 constant_dynamic-slice_fusion.5
  179.5 1.1 fusion.121
  180.7 0.6 constant_dynamic-slice_fusion.5
  183.3 1.1 fusion.121
  184.5 33.1 %while.34 = (s32[]{:T(128)}, f32[1,256,256]{2,1,0:T(8,128)S(1)}, f32[1,256]{1,0:T(1,128)S(1)}, f32[1]{0:T(128)}, f32[4,1,128,256]{3,2,1,0:T(8,128)S(1)}, /*index...) while((s32[]{:T(128)}, f32[1,256,256]{2,1,0:T(8,128)S(1)}, ...), condition=%wide.region_12.13_spmd, body=%wide.region_6.12_spmd.sunk | while | flops 219137792 | bytes 1794273 | solution.py:148
  184.8 0.6 slice.31
  185.4 1.3 fusion.113
  188.0 0.7 exponential_multiply_fusion.3
  188.7 1.0 fusion.117
  190.0 1.0 fusion.119
  190.9 1.2 fusion.120
  193.7 1.3 fusion.113
  196.2 0.7 exponential_multiply_fusion.3
  197.0 1.0 fusion.117
  198.2 1.0 fusion.119
  199.2 1.2 fusion.120
  201.9 1.3 fusion.113
  204.5 0.7 exponential_multiply_fusion.3
  205.3 1.0 fusion.117
  206.5 1.0 fusion.119
  207.5 1.2 fusion.120
  210.2 1.3 fusion.113
  212.8 0.7 exponential_multiply_fusion.3
  213.6 1.0 fusion.117
  214.8 1.0 fusion.119
  215.8 1.2 fusion.120
  217.6 5.5 %fusion.46 = f32[768,512]{1,0:T(8,128)} fusion(bf16[768,2048]{1,0:T(8,128)(2,1)} %bitcast.46, bf16[1,2048,512]{2,1,0:T(8,128)(2,1)} %param.35), kind=kOutput, calls=%fused_computation.71 | convolution fusion | flops 1610612736 | bytes 6815744 | tf_op jit(solution)/shard_map/dot_general | solution.py:183
  223.1 8.2 %convolution_convert_fusion = bf16[768,2048]{1,0:T(8,128)(2,1)} fusion(bf16[1,512,2048]{2,1,0:T(8,128)(2,1)S(1)} %copy-done, f32[768,512]{1,0:T(8,128)} %fusion.46, bf16[768,2048]{1,0:T(8,128)(2,1)} %bitcast.46, bf16[1,2048,512]{2,1,0:T(8,128)(2,1)} %param.36), kind=kOutput, calls=%fused_computation.64 | convolution fusion | flops 3225157632 | bytes 12058624 | tf_op jit(solution)/shard_map/dot_general | solution.py:186
  231.3 4.6 %all-to-all-start.1 = ((bf16[8,96,2048]{2,1,0:T(8,128)(2,1)}), bf16[8,96,2048]{2,1,0:T(8,128)(2,1)}, u32[]{:S(2)}, u32[]{:S(2)}) async-start(bf16[8,96,2048]{2,1,0:T(8,128)(2,1)} %bitcast.225), calls=%async_computation.2 | async-start | bytes 6291456 | tf_op jit(solution)/shard_map/all_to_all | solution.py:188
  236.1 3.3 %convolution_convert_fusion.2 = bf16[512,2048]{1,0:T(8,128)(2,1)} fusion(bf16[512,256]{1,0:T(8,128)(2,1)S(1)} %fusion.64, bf16[1024,2048]{1,0:T(8,128)(2,1)} %param.28, s32[]{:T(128)S(6)} %select_n.82), kind=kOutput, calls=%fused_computation.67 | convolution fusion | flops 537919488 | bytes 3407876 | tf_op jit(solution)/shard_map/dot_general | solution.py:155
  240.3 31.5 %reduce-scatter.2.cloned.1.call-done = bf16[128,2048]{1,0:T(8,128)(2,1)} async-done(((bf16[512,2048]{1,0:T(8,128)(2,1)}), bf16[128,2048]{1,0:T(8,128)(2,1)}) %reduce-scatter.2.cloned.1.call-update) | async-done | bytes 524304 | tf_op jit(solution)/shard_map/reduce_scatter | solution.py:154
  271.9 1.2 fusion.54
  273.1 2.0 fusion.56
  275.2 25.4 %all-to-all-done.1 = bf16[8,96,2048]{2,1,0:T(8,128)(2,1)} async-done(((bf16[8,96,2048]{2,1,0:T(8,128)(2,1)}), bf16[8,96,2048]{2,1,0:T(8,128)(2,1)}, u32[]{:S(2)}, u32[]{:S(2)}) %all-to-all-start.1) | async-done | bytes 3145760 | tf_op jit(solution)/shard_map/all_to_all | solution.py:188
  300.6 7.3 %gather_fusion = bf16[384,2048]{1,0:T(8,128)(2,1)} fusion(bf16[768,2048]{1,0:T(8,128)(2,1)} %bitcast.51, s32[1024]{0:T(1024)S(1)} %pad_clamp_fusion), kind=kCustom, calls=%fused_computation | custom fusion | bytes 3147264 | tf_op jit(solution)/shard_map/gather | solution.py:189
  307.9 4.7 %reshape.522 = f32[192,2,2048]{2,1,0:T(2,128)} reshape(bf16[384,2048]{1,0:T(8,128)(2,1)} %gather_fusion) | data formatting | bytes 4718592 | tf_op jit(solution)/shard_map/convert_element_type | solution.py:193
  312.7 7.8 %multiply_reduce_fusion = bf16[192,2048]{1,0:T(8,128)(2,1)} fusion(f32[192,2,2048]{2,1,0:T(2,128)} %reshape.522, f32[192,2]{1,0:T(8,128)S(1)} %copy.33), kind=kLoop, calls=%fused_computation.66 | loop fusion | flops 1179648 | bytes 3933696 | tf_op jit(solution)/shard_map/reduce_sum | solution.py:193
  (105 shorter events, 10.7 us)
Async XLA Ops:
  7.2 215.9 %copy-start = (bf16[1,512,2048]{2,1,0:T(8,128)(2,1)S(1)}, bf16[1,512,2048]{2,1,0:T(8,128)(2,1)}, u32[]{:S(2)}) copy-start(bf16[1,512,2048]{2,1,0:T(8,128)(2,1)} %param.37) | copy-start | bytes 6291460
  7.2 11.3 %copy-start.10 = (u32[32]{0:T(128)S(1)}, u32[32]{0:T(128)}, u32[]{:S(2)}) copy-start(u32[32]{0:T(128)} %constant.112) | copy-start | bytes 388
  7.2 14.8 %copy-start.3 = (bf16[192,2048]{1,0:T(8,128)(2,1)S(1)}, bf16[192,2048]{1,0:T(8,128)(2,1)}, u32[]{:S(2)}) copy-start(bf16[192,2048]{1,0:T(8,128)(2,1)} %param.30) | copy-start | bytes 2359300
  7.2 15.0 %copy-start.6 = (f32[2048]{0:T(1024)S(1)}, f32[2048]{0:T(1024)}, u32[]{:S(2)}) copy-start(f32[2048]{0:T(1024)} %param.31) | copy-start | bytes 24580
  7.2 144.5 %all-gather.5.cloned.1.call-start = ((), (), s32[]{:S(2)}) async-start(), calls=%async_computation.4 | async-start | bytes 2359296 | tf_op jit(solution)/shard_map/all_gather | solution.py:16
  25.0 94.3 %copy-start.1 = (bf16[512,256]{1,0:T(8,128)(2,1)S(1)}, bf16[512,256]{1,0:T(8,128)(2,1)}, u32[]{:S(2)}) copy-start(bf16[512,256]{1,0:T(8,128)(2,1)} %param.22) | copy-start | bytes 786436
  25.0 192.6 %all-to-all-start = ((bf16[8,96,2048]{2,1,0:T(8,128)(2,1)}), bf16[8,96,2048]{2,1,0:T(8,128)(2,1)}, u32[]{:S(2)}, u32[]{:S(2)}) async-start(bf16[8,96,2048]{2,1,0:T(8,128)(2,1)} %bitcast.221), calls=%async_computation.1 | async-start | bytes 6291456 | tf_op jit(solution)/shard_map/all_to_all | solution.py:181
  154.6 29.8 %copy-start.2 = (bf16[512,256]{1,0:T(8,128)(2,1)S(1)}, bf16[512,256]{1,0:T(8,128)(2,1)}, u32[]{:S(2)}) copy-start(bf16[512,256]{1,0:T(8,128)(2,1)} %param.23) | copy-start | bytes 786436
  154.6 29.8 %copy-start.4 = (f32[1,512]{1,0:T(1,128)S(1)}, f32[1,512]{1,0:T(1,128)}, u32[]{:S(2)}) copy-start(f32[1,512]{1,0:T(1,128)} %param.24) | copy-start | bytes 6148
  231.3 4.8 %copy-start.8 = (f32[256]{0:T(256)S(1)}, f32[256]{0:T(256)}, u32[]{:S(2)}) copy-start(f32[256]{0:T(256)} %param.27) | copy-start | bytes 3076
  231.3 69.3 %all-to-all-start.1 = ((bf16[8,96,2048]{2,1,0:T(8,128)(2,1)}), bf16[8,96,2048]{2,1,0:T(8,128)(2,1)}, u32[]{:S(2)}, u32[]{:S(2)}) async-start(bf16[8,96,2048]{2,1,0:T(8,128)(2,1)} %bitcast.225), calls=%async_computation.2 | async-start | bytes 6291456 | tf_op jit(solution)/shard_map/all_to_all | solution.py:188
  235.8 36.0 %reduce-scatter.2.cloned.1.call-start = ((), (), s32[]{:S(2)}) async-start(), calls=%async_computation.3 | async-start | bytes 2621440 | tf_op jit(solution)/shard_map/reduce_scatter | solution.py:154
  239.4 0.7 copy-start.5
  239.4 0.7 copy-start.9
  239.4 33.7 %copy-start.7 = (f32[2048]{0:T(1024)S(1)}, f32[2048]{0:T(1024)}, u32[]{:S(2)}) copy-start(f32[2048]{0:T(1024)} %param.29) | copy-start | bytes 24580
Sparse Core Ops, SparseCore 0:
  16.0 102.3 all-gather.4
  239.6 32.2 reduce-scatter.1
where the time goes:
time: 329 us; the launch traced here: 327 us
  blocking collectives  119 us (36%)
  waiting for transfers between devices  57 us (17%)
  matrix products  37.5 us (11%)
  other arithmetic  37.2 us (11%)
  local copies, waits for them, and re-layouts  28.6 us (9%)
  loops' own time  21.4 us (7%)
  between operations  14.3 us (4%)
  starting transfers between devices  12.2 us (4%)
    unnamed x1, blocking collectives  86.9 us
    all_gather x1, blocking collectives, entering_2(): everything = jax.tree.map(lambda part: lax.all_gather(part, axis), array)  32.2 us
    reduce_scatter x1, waiting for transfers between devices, shards(): lax.psum_scatter(jnp.dot(head_out, weight_rows, preferred_element_type=jn...  31.5 us
    all_to_all x1, waiting for transfers between devices, shards(): lax.all_to_all(answers, 'ep', split_axis=0, concat_axis=0, tiled=True)  25.4 us
    another operation x1, loops' own time, entering_2(): return lax.fori_loop(0, devices, step, start)  15.8 us
    select_n x16, other arithmetic, step(): return jax.tree.map(lambda a, b: jnp.where(reached, a, b), new, before)  9.28 us
    dot_general x1, matrix products, shards(): jnp.dot(hidden, w_down, preferred_element_type=jnp.float32)  8.18 us
    reduce_sum x1, other arithmetic, shards(): jnp.sum(route_weight[:, :, None] * picked.astype(jnp.float32), axis=1)  7.76 us
  transfers between devices with their start and end apart: 4, of which 2 were waited for; matrix products, arithmetic and copies ran while one was open for 19% of the time, Pallas kernels for 0%

commit v1 on v0

v1 whole, which is shorter than its diff:
```python
import functools

import jax
import jax.numpy as jnp
from jax import lax
from jax.experimental import pallas as pl
from jax.experimental.pallas import tpu as pltpu
from jax.sharding import PartitionSpec as P

FLOOR = -1e30
EPS = 1e-06
MESH = pl.DeviceIdType.MESH
F32 = jnp.float32
BF16 = jnp.bfloat16


def rms(values, gain):
    squares = jnp.mean(values * values, axis=-1, keepdims=True)
    return values * lax.rsqrt(squares + EPS) * gain


def dot(a, b, dims=((1,), (0,)), precision=None):
    return lax.dot_general(a, b, (dims, ((), ())), preferred_element_type=F32, precision=precision)


def join(early, late):
    total_e, peak_e, mem_e, nor_e = early
    total_l, peak_l, mem_l, nor_l = late
    peak = jnp.maximum(total_l + peak_e, peak_l)
    fe = jnp.exp(total_l + peak_e - peak)
    fl = jnp.exp(peak_l - peak)
    return (total_e + total_l, peak, fe * mem_e + fl * mem_l, fe * nor_e + fl * nor_l)


def kernel(
    n, nt, cap,
    q_ref, k_ref, v_ref, ig_ref, fg_ref, fb_ref, hs_ref, wo_hbm, ps_ref,
    x_ref, es_ref, ids_ref, grp_ref, sc_ref, wg_hbm, wu_hbm, wd_hbm,
    mixed_ref, routed_ref,
    wg, wu, wd, wo, out, recv, ans, back, ffn, acc,
    cpair, spair, cgrp, sgrp, ent, head, pout, prec,
    wsem, d_ss, d_rs, a_ss, a_rs, c1s, c1r, s1s, s1r, c2s, c2r, s2s, s2r, p_ss, p_rs,
):
    me = lax.axis_index("ep")
    tp = lax.axis_index("tp")
    groups = n // 2
    grp = me // 2
    par = lax.rem(me, 2)
    partner = me + 1 - 2 * par
    tokens, width = x_ref.shape
    length, hd = q_ref.shape
    rows = mixed_ref.shape[0]

    barrier = pltpu.get_barrier_semaphore()

    def greet(i, c):
        pl.semaphore_signal(barrier, inc=1, device_id=(lax.rem(me + i, n), tp), device_id_type=MESH)
        return c

    lax.fori_loop(1, n, greet, 0)
    for j in range(1, nt):
        pl.semaphore_signal(barrier, inc=1, device_id=(me, lax.rem(tp + j, nt)), device_id_type=MESH)

    loads = [
        pltpu.make_async_copy(wg_hbm.at[0], wg, wsem.at[0]),
        pltpu.make_async_copy(wu_hbm.at[0], wu, wsem.at[1]),
        pltpu.make_async_copy(wd_hbm.at[0], wd, wsem.at[2]),
        pltpu.make_async_copy(wo_hbm.at[pl.ds(pl.multiple_of(tp * hd, hd), hd)], wo, wsem.at[3]),
    ]
    for load in loads:
        load.start()

    fg = fg_ref[...]
    lk = jnp.minimum(fg, 0.0) - jnp.log1p(jnp.exp(-jnp.abs(fg))) + fb_ref[...]
    rid = lax.broadcasted_iota(jnp.int32, (length, length), 0)
    cid = lax.broadcasted_iota(jnp.int32, (length, length), 1)
    upper = (rid <= cid).astype(F32)
    b_row = dot(jnp.broadcast_to(lk, (8, length)), upper, precision=lax.Precision.HIGHEST)[0:1]
    i_row = ig_ref[...]
    last = b_row[:, length - 1 : length]
    g_row = last - b_row + i_row
    m_loc = jnp.max(g_row, axis=-1, keepdims=True)
    which = lax.broadcasted_iota(jnp.int32, (128, length), 0)
    cols = jnp.where(which == 0, b_row, g_row).T
    b_col = cols[:, 0:1]
    g_col = cols[:, 1:2]
    kw = k_ref[...].astype(F32) * (jnp.exp(g_col - m_loc) * (hd**-0.5))
    c_loc = dot(kw.astype(BF16), v_ref[...], ((0,), (0,)))
    n_loc = jnp.sum(kw, axis=0, keepdims=True)
    stat_id = lax.broadcasted_iota(jnp.int32, (8, hd), 0)

    def stats(total, peak, nor):
        return jnp.where(stat_id == 0, nor, jnp.where(stat_id == 1, peak, total))

    cpair[par] = c_loc.astype(BF16)
    spair[par] = stats(last, m_loc, n_loc)

    pl.semaphore_wait(barrier, n - 1 + nt - 1)

    def pair_copies():
        return [
            pltpu.make_async_remote_copy(
                src_ref=cpair.at[par], dst_ref=cpair.at[par], send_sem=c1s, recv_sem=c1r,
                device_id=(partner, tp), device_id_type=MESH),
            pltpu.make_async_remote_copy(
                src_ref=spair.at[par], dst_ref=spair.at[par], send_sem=s1s, recv_sem=s1r,
                device_id=(partner, tp), device_id_type=MESH),
        ]

    for copy in pair_copies():
        copy.start()

    ffn[...] = rms(x_ref[...].astype(F32), es_ref[...]).astype(BF16)
    ids = ids_ref[...]
    first, second = ids[:, 0:1], ids[:, 1:2]
    lane_e = lax.broadcasted_iota(jnp.int32, (tokens, n), 1)
    named = ((lane_e == first) | (lane_e == second)).astype(F32)
    tr = lax.broadcasted_iota(jnp.int32, (tokens, tokens), 0)
    tc = lax.broadcasted_iota(jnp.int32, (tokens, tokens), 1)
    rank = dot((tc < tr).astype(BF16), named.astype(BF16))
    slot_a = first * cap + jnp.sum(jnp.where(lane_e == first, rank, 0.0), axis=1, keepdims=True).astype(jnp.int32)
    slot_b = second * cap + jnp.sum(jnp.where(lane_e == second, rank, 0.0), axis=1, keepdims=True).astype(jnp.int32)
    score = sc_ref[...]
    ex = jnp.exp(score - jnp.max(score, axis=-1, keepdims=True))
    route = grp_ref[...] * (ex / jnp.sum(ex, axis=-1, keepdims=True))
    rw_a, rw_b = route[:, 0:1], route[:, 1:2]
    lane_c = lax.broadcasted_iota(jnp.int32, (tokens, cap), 1)

    def pack(e):
        lane = lane_c + e * cap
        place = ((lane == slot_a) | (lane == slot_b)).astype(BF16)
        out[e] = dot(place, ffn[...], ((0,), (0,))).astype(BF16)

    def offset(i):
        return n // 2 + jnp.where(lax.rem(i, 2) == 0, i // 2, -((i + 1) // 2))

    def dispatch_copy(e):
        return pltpu.make_async_remote_copy(
            src_ref=out.at[e], dst_ref=recv.at[me], send_sem=d_ss.at[e], recv_sem=d_rs.at[me],
            device_id=(e, tp), device_id_type=MESH)

    def dispatch_arrival(s):
        return pltpu.make_async_remote_copy(
            src_ref=out.at[s], dst_ref=recv.at[s], send_sem=d_ss.at[s], recv_sem=d_rs.at[s],
            device_id=(s, tp), device_id_type=MESH)

    def answer_copy(s):
        return pltpu.make_async_remote_copy(
            src_ref=ans.at[s], dst_ref=back.at[me], send_sem=a_ss.at[s], recv_sem=a_rs.at[me],
            device_id=(s, tp), device_id_type=MESH)

    def answer_arrival(e):
        return pltpu.make_async_remote_copy(
            src_ref=ans.at[e], dst_ref=back.at[e], send_sem=a_ss.at[e], recv_sem=a_rs.at[e],
            device_id=(e, tp), device_id_type=MESH)

    for copy in pair_copies():
        copy.wait_send()
    def pair_arrival():
        return [
            pltpu.make_async_remote_copy(
                src_ref=cpair.at[1 - par], dst_ref=cpair.at[1 - par], send_sem=c1s, recv_sem=c1r,
                device_id=(partner, tp), device_id_type=MESH),
            pltpu.make_async_remote_copy(
                src_ref=spair.at[1 - par], dst_ref=spair.at[1 - par], send_sem=s1s, recv_sem=s1r,
                device_id=(partner, tp), device_id_type=MESH),
        ]

    for copy in pair_arrival():
        copy.wait_recv()

    def unpack(c, s):
        return (s[2:3], s[1:2], c.astype(F32), s[0:1])

    both = join(unpack(cpair[0], spair[0]), unpack(cpair[1], spair[1]))
    cgrp[grp] = both[2].astype(BF16)
    sgrp[grp] = stats(both[0], both[1], both[3])

    def group_copies(g):
        to = (g * 2 + par, tp)
        return [
            pltpu.make_async_remote_copy(
                src_ref=cgrp.at[grp], dst_ref=cgrp.at[grp], send_sem=c2s.at[g], recv_sem=c2r.at[grp],
                device_id=to, device_id_type=MESH),
            pltpu.make_async_remote_copy(
                src_ref=sgrp.at[grp], dst_ref=sgrp.at[grp], send_sem=s2s.at[g], recv_sem=s2r.at[grp],
                device_id=to, device_id_type=MESH),
        ]

    def group_arrivals(g):
        at = (g * 2 + par, tp)
        return [
            pltpu.make_async_remote_copy(
                src_ref=cgrp.at[g], dst_ref=cgrp.at[g], send_sem=c2s.at[g], recv_sem=c2r.at[g],
                device_id=at, device_id_type=MESH),
            pltpu.make_async_remote_copy(
                src_ref=sgrp.at[g], dst_ref=sgrp.at[g], send_sem=s2s.at[g], recv_sem=s2r.at[g],
                device_id=at, device_id_type=MESH),
        ]

    def send_group(g, c):
        for copy in group_copies(g):
            copy.start()
        return c

    lax.fori_loop(grp + 1, groups, send_group, 0)

    def send_tokens(i, c):
        e = lax.rem(me + offset(i), n)
        pack(e)
        dispatch_copy(e).start()
        return c

    lax.fori_loop(0, n - 1, send_tokens, 0)
    pack(me)
    for load in loads:
        load.wait()

    def expert(chosen):
        gate = dot(chosen, wg[...])
        up = dot(chosen, wu[...])
        hidden = (gate / (1.0 + jnp.exp(-gate)) * up).astype(BF16)
        return dot(hidden, wd[...]).astype(BF16)

    ans[me] = expert(out[me])

    ent[...] = jnp.zeros(ent.shape, F32)
    row1 = jnp.zeros((1, hd), F32)

    def enter(g, carry):
        total, peak, nor = carry
        for copy in group_arrivals(g):
            copy.wait_recv()
        total, peak, mem, nor = join((total, peak, ent[...], nor), unpack(cgrp[g], sgrp[g]))
        ent[...] = mem
        return total, peak, nor

    total, peak, nor = lax.fori_loop(0, grp, enter, (row1, row1 + FLOOR, row1))
    joined = join((total, peak, ent[...], nor), unpack(cpair[0], spair[0]))
    odd = par == 1
    m_in = jnp.where(odd, joined[1], peak)
    n_in = jnp.where(odd, joined[3], nor)
    c_in = jnp.where(odd, joined[2], ent[...])

    carried = b_col + m_in[:, 0:1]
    decay = jnp.where(cid <= rid, b_col - b_row + i_row, -jnp.inf)
    peaks = jnp.maximum(carried, jnp.max(decay, axis=-1, keepdims=True))
    across = jnp.exp(carried - peaks)
    scores = dot(q_ref[...], k_ref[...], ((1,), (1,))) * (hd**-0.5) * jnp.exp(decay - peaks)
    qf = q_ref[...].astype(F32)
    den = jnp.sum(scores, axis=-1, keepdims=True) + across * jnp.sum(qf * n_in, axis=-1, keepdims=True)
    num = dot(scores.astype(BF16), v_ref[...]) + across * dot(q_ref[...], c_in.astype(BF16))
    cell = num / jnp.maximum(jnp.abs(den), jnp.exp(-peaks))
    head[...] = (cell * hs_ref[...]).astype(BF16)

    def part_copy(j):
        return pltpu.make_async_remote_copy(
            src_ref=pout.at[j], dst_ref=prec.at[tp], send_sem=p_ss.at[j], recv_sem=p_rs.at[tp],
            device_id=(me, j), device_id_type=MESH)

    def part_arrival(j):
        return pltpu.make_async_remote_copy(
            src_ref=pout.at[j], dst_ref=prec.at[j], send_sem=p_ss.at[j], recv_sem=p_rs.at[j],
            device_id=(me, j), device_id_type=MESH)

    def project(j):
        pout[j] = dot(head[pl.ds(pl.multiple_of(j * rows, rows), rows), :], wo[...]).astype(BF16)

    def send_part(i, c):
        j = lax.rem(tp + i, nt)
        project(j)
        part_copy(j).start()
        return c

    lax.fori_loop(1, nt, send_part, 0)
    project(tp)

    def serve(i, c):
        s = lax.rem(me - offset(i) + n, n)
        dispatch_arrival(s).wait_recv()
        ans[s] = expert(recv[s])
        answer_copy(s).start()
        return c

    lax.fori_loop(0, n - 1, serve, 0)

    def mix(i, total):
        j = lax.rem(tp + i, nt)
        part_arrival(j).wait_recv()
        return total + prec[j].astype(F32)

    projected = pout[tp].astype(F32)
    for i in range(1, nt):
        projected = mix(i, projected)
    mixed_ref[...] = rms(projected, ps_ref[...]).astype(BF16)

    def weigh(e, block):
        lane = lane_c + e * cap
        w = jnp.where(lane == slot_a, rw_a, jnp.where(lane == slot_b, rw_b, 0.0))
        high = w.astype(BF16)
        low = (w - high.astype(F32)).astype(BF16)
        return dot(high, block) + dot(low, block)

    acc[...] = weigh(me, ans[me])

    def collect(i, c):
        e = lax.rem(me + offset(i), n)
        answer_arrival(e).wait_recv()
        acc[...] += weigh(e, back[e])
        return c

    lax.fori_loop(0, n - 1, collect, 0)
    routed_ref[...] = acc[...].astype(BF16)

    def finish(i, c):
        e = lax.rem(me + i, n)
        dispatch_copy(e).wait_send()
        answer_copy(e).wait_send()
        return c

    lax.fori_loop(1, n, finish, 0)

    def finish_group(g, c):
        for copy in group_copies(g):
            copy.wait_send()
        return c

    lax.fori_loop(grp + 1, groups, finish_group, 0)
    for i in range(1, nt):
        part_copy(lax.rem(tp + i, nt)).wait_send()


def shards(
    n, nt,
    memory_query_matrix, memory_key_matrix, memory_value_matrix,
    input_gate_logits, forget_gate_logits, forget_log_boosts,
    head_norm_scale, memory_output_matrix, projection_norm_scale,
    second_batch_rows, expert_prenorm_scale, selected_expert_index,
    group_route_probability, expert_choice_scores,
    expert_gate_matrix, expert_up_matrix, expert_down_matrix,
):
    length, hd = memory_query_matrix.shape
    tokens, width = second_batch_rows.shape
    hidden = expert_gate_matrix.shape[2]
    cap = 2 * selected_expert_index.shape[1] * tokens // n
    cap = -(-cap // 16) * 16
    rows = length // nt
    vm = pl.BlockSpec(memory_space=pltpu.VMEM)
    hbm = pl.BlockSpec(memory_space=pl.ANY)
    dma = pltpu.SemaphoreType.DMA
    slots = pltpu.VMEM((n, cap, width), BF16)
    return pl.pallas_call(
        functools.partial(kernel, n, nt, cap),
        out_shape=(
            jax.ShapeDtypeStruct((rows, width), BF16),
            jax.ShapeDtypeStruct((tokens, width), BF16),
        ),
        in_specs=[vm] * 7 + [hbm] + [vm] * 6 + [hbm] * 3,
        out_specs=(vm, vm),
        scratch_shapes=[
            pltpu.VMEM((width, hidden), BF16),
            pltpu.VMEM((width, hidden), BF16),
            pltpu.VMEM((hidden, width), BF16),
            pltpu.VMEM((hd, width), BF16),
            slots, slots, slots, slots,
            pltpu.VMEM((tokens, width), BF16),
            pltpu.VMEM((tokens, width), F32),
            pltpu.VMEM((2, hd, hd), BF16),
            pltpu.VMEM((2, 8, hd), F32),
            pltpu.VMEM((n // 2, hd, hd), BF16),
            pltpu.VMEM((n // 2, 8, hd), F32),
            pltpu.VMEM((hd, hd), F32),
            pltpu.VMEM((length, hd), BF16),
            pltpu.VMEM((nt, rows, width), BF16),
            pltpu.VMEM((nt, rows, width), BF16),
            dma((4,)),
            dma((n,)), dma((n,)), dma((n,)), dma((n,)),
            dma, dma, dma, dma,
            dma((n // 2,)), dma((n // 2,)), dma((n // 2,)), dma((n // 2,)),
            dma((nt,)), dma((nt,)),
        ],
        compiler_params=pltpu.CompilerParams(
            collective_id=0, has_side_effects=True, vmem_limit_bytes=62 * 1024 * 1024
        ),
    )(
        memory_query_matrix, memory_key_matrix, memory_value_matrix,
        input_gate_logits, forget_gate_logits, forget_log_boosts,
        head_norm_scale[None], memory_output_matrix, projection_norm_scale[None],
        second_batch_rows, expert_prenorm_scale[None], selected_expert_index,
        group_route_probability[:, None], expert_choice_scores,
        expert_gate_matrix, expert_up_matrix, expert_down_matrix,
    )


def solution(mesh):
    return jax.shard_map(
        functools.partial(shards, mesh.shape["ep"], mesh.shape["tp"]),
        mesh=mesh,
        in_specs=(
            P("ep", "tp"), P("ep", "tp"), P("ep", "tp"),
            P("tp", "ep"), P("tp", "ep"), P("tp", "ep"),
            P("tp"), P(), P(),
            P(("ep", "tp"), None), P(), P(("ep", "tp"), None),
            P(("ep", "tp")), P(("ep", "tp"), None),
            P("ep", None, None), P("ep", None, None), P("ep", None, None),
        ),
        out_specs=(P(("ep", "tp"), None), P(("ep", "tp"), None)),
        check_vma=False,
    )
```

time: 329 us -> 169 us (0.51)
  the two profiles are of different devices: /device:TPU:0 before, /device:TPU:16 now
where the time goes in v1:
time: 169 us
  Pallas kernels  160 us (95%)
  local copies, waits for them, and re-layouts  8.3 us (5%)
    pallas_call x1, Pallas kernels, shards(): pl.pallas_call(functools.partial(kernel, n, nt, cap), out_shape=(jax.Shap...  160 us
    unnamed x4, local copies, waits for them, and re-layouts  6.86 us

profile of v1, /device:TPU:16, one launch (start us, length us, event | category | flops | bytes accessed | tf_op | source)
XLA Modules:
  0.0 168.6 jit_solution(16570706669987493474)
XLA Ops:
  0.6 1.4 copy.21.ids_ref
  2.1 1.4 copy.22.grp_ref
  3.5 1.4 copy.23.sc_ref
  5.0 159.7 %shard_map.176 = (bf16[128,2048]{1,0:T(8,128)(2,1)}, bf16[192,2048]{1,0:T(8,128)(2,1)}) custom-call(bf16[512,256]{1,0:T(8,128)(2,1)} %q_ref.1, bf16[512,256]{1,0:T(8,128)(2,1)} %k_ref.1, bf16[512,256]{1,0:T(8,128)(2,1)} %v_ref.1, f32[1,512]{1,0:T(1,128)} %ig_ref.1, f32[1,512]{1,0:T(1,128)} %fg_ref.1, f32[1,512]{1,0:T(1,128)} %fb_ref.1, f32[1,256]{1,0:T(1,128)} %bitcast.7, ...), custom_call_target="tpu_custom_call" | custom-call | tf_op jit(solution)/shard_map/pallas_call | solution.py:352
  164.7 1.9 %copy.26 = bf16[128,2048]{1,0:T(8,128)(2,1)} copy(bf16[128,2048]{1,0:T(8,128)(2,1)} %get-tuple-element.4) | data formatting | bytes 1048576
  166.5 2.1 %copy.27 = bf16[192,2048]{1,0:T(8,128)(2,1)} copy(bf16[192,2048]{1,0:T(8,128)(2,1)} %get-tuple-element.5) | data formatting | bytes 1572864

commit v2 on v1

--- a/solution.py
+++ b/solution.py
@@ -319,6 +319,421 @@
         return c
 
     lax.fori_loop(1, n, finish, 0)
+
+    def finish_group(g, c):
+        for copy in group_copies(g):
+            copy.wait_send()
+        return c
+
+    lax.fori_loop(grp + 1, groups, finish_group, 0)
+    for i in range(1, nt):
+        part_copy(lax.rem(tp + i, nt)).wait_send()
+
+
+def relay_kernel(
+    n, nt, cap,
+    q_ref, k_ref, v_ref, ig_ref, fg_ref, fb_ref, hs_ref, wo_hbm, ps_ref,
+    x_ref, es_ref, ids_ref, grp_ref, sc_ref, wg_hbm, wu_hbm, wd_hbm,
+    mixed_ref, routed_ref,
+    wg, wu, wd, wo, tok, info, xs, xr, ya, yb, own, part, ret, acc,
+    cpair, spair, cgrp, sgrp, ent, head, pout, prec,
+    wsem, t_ss, t_rs, i_ss, i_rs, x_ss, x_rs, y_ss, y_rs, r_ss, r_rs, c1s, c1r, s1s, s1r, c2s, c2r, s2s, s2r, p_ss, p_rs,
+):
+    me = lax.axis_index("ep")
+    tp = lax.axis_index("tp")
+    groups = n // 2
+    grp = me // 2
+    par = lax.rem(me, 2)
+    partner = me + 1 - 2 * par
+    tokens, width = x_ref.shape
+    length, hd = q_ref.shape
+    rows = mixed_ref.shape[0]
+
+    barrier = pltpu.get_barrier_semaphore()
+
+    def greet(i, c):
+        pl.semaphore_signal(barrier, inc=1, device_id=(lax.rem(me + i, n), tp), device_id_type=MESH)
+        return c
+
+    lax.fori_loop(1, n, greet, 0)
+    for j in range(1, nt):
+        pl.semaphore_signal(barrier, inc=1, device_id=(me, lax.rem(tp + j, nt)), device_id_type=MESH)
+
+    loads = [
+        pltpu.make_async_copy(wg_hbm.at[0], wg, wsem.at[0]),
+        pltpu.make_async_copy(wu_hbm.at[0], wu, wsem.at[1]),
+        pltpu.make_async_copy(wd_hbm.at[0], wd, wsem.at[2]),
+        pltpu.make_async_copy(wo_hbm.at[pl.ds(pl.multiple_of(tp * hd, hd), hd)], wo, wsem.at[3]),
+    ]
+    for load in loads:
+        load.start()
+
+    tok[grp] = rms(x_ref[...].astype(F32), es_ref[...]).astype(BF16)
+    half = tokens // 2
+
+    def tok_copy(s, h, to, sem):
+        rows_of = pl.ds(h * half, half)
+        return pltpu.make_async_remote_copy(
+            src_ref=tok.at[s, rows_of], dst_ref=tok.at[s, rows_of], send_sem=t_ss.at[sem, h],
+            recv_sem=t_rs.at[s, h], device_id=(to * 2 + par, tp), device_id_type=MESH)
+
+    def info_copy(g, s):
+        return pltpu.make_async_remote_copy(
+            src_ref=info.at[s], dst_ref=info.at[s], send_sem=i_ss.at[g],
+            recv_sem=i_rs.at[s], device_id=(g * 2 + par, tp), device_id_type=MESH)
+
+    def swap_copy(kind, s):
+        src, dst, ss, rs = ((xs, xr, x_ss, x_rs), (ya, yb, y_ss, y_rs))[kind]
+        return pltpu.make_async_remote_copy(
+            src_ref=src.at[s], dst_ref=dst.at[s], send_sem=ss.at[s],
+            recv_sem=rs.at[s], device_id=(partner, tp), device_id_type=MESH)
+
+    def ret_copy(s, slot, to):
+        return pltpu.make_async_remote_copy(
+            src_ref=part.at[s], dst_ref=ret.at[slot], send_sem=r_ss.at[s],
+            recv_sem=r_rs.at[slot], device_id=(to * 2 + par, tp), device_id_type=MESH)
+
+
+    pl.semaphore_wait(barrier, n - 1 + nt - 1)
+    for h in range(2):
+        @pl.when(grp + 1 < groups)
+        def _():
+            tok_copy(grp, h, grp + 1, grp).start()
+
+        @pl.when(grp > 0)
+        def _():
+            tok_copy(grp, h, grp - 1, groups).start()
+
+    ids = ids_ref[...]
+    first, second = ids[:, 0:1], ids[:, 1:2]
+    lane_e = lax.broadcasted_iota(jnp.int32, (tokens, n), 1)
+    named = ((lane_e == first) | (lane_e == second)).astype(F32)
+    tr = lax.broadcasted_iota(jnp.int32, (tokens, tokens), 0)
+    tc = lax.broadcasted_iota(jnp.int32, (tokens, tokens), 1)
+    rank = dot((tc < tr).astype(BF16), named.astype(BF16))
+    slot_a = first * cap + jnp.sum(jnp.where(lane_e == first, rank, 0.0), axis=1, keepdims=True).astype(jnp.int32)
+    slot_b = second * cap + jnp.sum(jnp.where(lane_e == second, rank, 0.0), axis=1, keepdims=True).astype(jnp.int32)
+    score = sc_ref[...]
+    ex = jnp.exp(score - jnp.max(score, axis=-1, keepdims=True))
+    route = grp_ref[...] * (ex / jnp.sum(ex, axis=-1, keepdims=True))
+    rw_a, rw_b = route[:, 0:1], route[:, 1:2]
+    lane_c = lax.broadcasted_iota(jnp.int32, (tokens, cap), 1)
+
+    lane_i = lax.broadcasted_iota(jnp.int32, (tokens, 128), 1)
+    table = jnp.where(lane_i == 0, slot_a.astype(F32), jnp.where(lane_i == 1, slot_b.astype(F32),
+        jnp.where(lane_i == 2, rw_a, jnp.where(lane_i == 3, rw_b, 0.0))))
+    wide = info.shape[2]
+    table = jnp.concatenate([table, jnp.zeros((wide - tokens, 128), F32)], axis=0)
+    info[grp] = table.T[0:8]
+
+    def send_info(j, c):
+        info_copy(lax.rem(grp + j, groups), grp).start()
+        return c
+
+    lax.fori_loop(1, groups, send_info, 0)
+
+    def columns(s):
+        wide_cols = jnp.concatenate([info[s], jnp.zeros((120, info.shape[2]), F32)], axis=0).T[0:tokens]
+        return (wide_cols[:, 0:1].astype(jnp.int32), wide_cols[:, 1:2].astype(jnp.int32),
+                wide_cols[:, 2:3], wide_cols[:, 3:4])
+
+    def place(cols_s, e):
+        lane = lane_c + e * cap
+        return ((lane == cols_s[0]) | (lane == cols_s[1])).astype(BF16)
+
+    def pack(s):
+        xs[s] = dot(place(columns(s), partner), tok[s], ((0,), (0,))).astype(BF16)
+        swap_copy(0, s).start()
+
+    pack(grp)
+
+    fg = fg_ref[...]
+    lk = jnp.minimum(fg, 0.0) - jnp.log1p(jnp.exp(-jnp.abs(fg))) + fb_ref[...]
+    rid = lax.broadcasted_iota(jnp.int32, (length, length), 0)
+    cid = lax.broadcasted_iota(jnp.int32, (length, length), 1)
+    upper = (rid <= cid).astype(F32)
+    b_row = dot(jnp.broadcast_to(lk, (8, length)), upper, precision=lax.Precision.HIGHEST)[0:1]
+    i_row = ig_ref[...]
+    last = b_row[:, length - 1 : length]
+    g_row = last - b_row + i_row
+    m_loc = jnp.max(g_row, axis=-1, keepdims=True)
+    which = lax.broadcasted_iota(jnp.int32, (128, length), 0)
+    cols = jnp.where(which == 0, b_row, g_row).T
+    b_col = cols[:, 0:1]
+    g_col = cols[:, 1:2]
+    kw = k_ref[...].astype(F32) * (jnp.exp(g_col - m_loc) * (hd**-0.5))
+    c_loc = dot(kw.astype(BF16), v_ref[...], ((0,), (0,)))
+    n_loc = jnp.sum(kw, axis=0, keepdims=True)
+    stat_id = lax.broadcasted_iota(jnp.int32, (8, hd), 0)
+
+    def stats(total, peak, nor):
+        return jnp.where(stat_id == 0, nor, jnp.where(stat_id == 1, peak, total))
+
+    cpair[par] = c_loc.astype(BF16)
+    spair[par] = stats(last, m_loc, n_loc)
+
+    def pair_copies():
+        return [
+            pltpu.make_async_remote_copy(
+                src_ref=cpair.at[par], dst_ref=cpair.at[par], send_sem=c1s, recv_sem=c1r,
+                device_id=(partner, tp), device_id_type=MESH),
+            pltpu.make_async_remote_copy(
+                src_ref=spair.at[par], dst_ref=spair.at[par], send_sem=s1s, recv_sem=s1r,
+                device_id=(partner, tp), device_id_type=MESH),
+        ]
+
+    for copy in pair_copies():
+        copy.start()
+
+    for copy in pair_copies():
+        copy.wait_send()
+    def pair_arrival():
+        return [
+            pltpu.make_async_remote_copy(
+                src_ref=cpair.at[1 - par], dst_ref=cpair.at[1 - par], send_sem=c1s, recv_sem=c1r,
+                device_id=(partner, tp), device_id_type=MESH),
+            pltpu.make_async_remote_copy(
+                src_ref=spair.at[1 - par], dst_ref=spair.at[1 - par], send_sem=s1s, recv_sem=s1r,
+                device_id=(partner, tp), device_id_type=MESH),
+        ]
+
+    for copy in pair_arrival():
+        copy.wait_recv()
+
+    def unpack(c, s):
+        return (s[2:3], s[1:2], c.astype(F32), s[0:1])
+
+    both = join(unpack(cpair[0], spair[0]), unpack(cpair[1], spair[1]))
+    cgrp[grp] = both[2].astype(BF16)
+    sgrp[grp] = stats(both[0], both[1], both[3])
+
+    def group_copies(g):
+        to = (g * 2 + par, tp)
+        return [
+            pltpu.make_async_remote_copy(
+                src_ref=cgrp.at[grp], dst_ref=cgrp.at[grp], send_sem=c2s.at[g], recv_sem=c2r.at[grp],
+                device_id=to, device_id_type=MESH),
+            pltpu.make_async_remote_copy(
+                src_ref=sgrp.at[grp], dst_ref=sgrp.at[grp], send_sem=s2s.at[g], recv_sem=s2r.at[grp],
+                device_id=to, device_id_type=MESH),
+        ]
+
+    def group_arrivals(g):
+        at = (g * 2 + par, tp)
+        return [
+            pltpu.make_async_remote_copy(
+                src_ref=cgrp.at[g], dst_ref=cgrp.at[g], send_sem=c2s.at[g], recv_sem=c2r.at[g],
+                device_id=at, device_id_type=MESH),
+            pltpu.make_async_remote_copy(
+                src_ref=sgrp.at[g], dst_ref=sgrp.at[g], send_sem=s2s.at[g], recv_sem=s2r.at[g],
+                device_id=at, device_id_type=MESH),
+        ]
+
+    def send_group(g, c):
+        for copy in group_copies(g):
+            copy.start()
+        return c
+
+    lax.fori_loop(grp + 1, groups, send_group, 0)
+
+    for load in loads:
+        load.wait()
+
+    def weigh(cols_s, e, block):
+        lane = lane_c + e * cap
+        w = jnp.where(lane == cols_s[0], cols_s[2], jnp.where(lane == cols_s[1], cols_s[3], 0.0))
+        high = w.astype(BF16)
+        low = (w - high.astype(F32)).astype(BF16)
+        return dot(high, block) + dot(low, block)
+
+    def experts(s):
+        cols_s = columns(s)
+        mine = dot(place(cols_s, me), tok[s], ((0,), (0,))).astype(BF16)
+        swap_copy(0, s).wait_recv()
+        chosen = jnp.concatenate([xr[s], mine], axis=0)
+        gate = dot(chosen, wg[...])
+        up = dot(chosen, wu[...])
+        hidden = (gate / (1.0 + jnp.exp(-gate)) * up).astype(BF16)
+        answer = dot(hidden, wd[...]).astype(BF16)
+        ya[s] = answer[0:cap]
+        swap_copy(1, s).start()
+        own[s] = answer[cap:]
+
+    def combined(s):
+        cols_s = columns(s)
+        swap_copy(1, s).wait_recv()
+        return weigh(cols_s, me, own[s]) + weigh(cols_s, partner, yb[s])
+
+    def hop(s):
+        below = s < grp
+        to = jnp.where(below, grp - 1, grp + 1)
+        slot = jnp.where(to == s, jnp.where(below, s, groups), s)
+        return ret_copy(s, slot, to)
+
+    def where_is(i):
+        d, side = 1 + i // 2, lax.rem(i, 2)
+        s = grp + d * (2 * side - 1)
+        return s, (s >= 0) & (s < groups)
+
+    def at_end(s):
+        return jnp.where(s < grp, grp == groups - 1, grp == 0)
+
+    def take(i, c):
+        s, valid = where_is(i)
+
+        @pl.when(valid)
+        def _():
+            onward = jnp.where(s < grp, grp + 1, grp - 1)
+            for h in range(2):
+                tok_copy(s, h, grp, s).wait_recv()
+
+                @pl.when(jnp.logical_not(at_end(s)))
+                def _():
+                    tok_copy(s, h, onward, s).start()
+
+            info_copy(s, s).wait_recv()
+            pack(s)
+
+        return c
+
+    def work(i, c):
+        s, valid = where_is(i)
+
+        @pl.when(valid)
+        def _():
+            experts(s)
+
+        return c
+
+    def close(i, c):
+        s, valid = where_is(i)
+
+        @pl.when(valid & at_end(s))
+        def _():
+            part[s] = combined(s).astype(BF16)
+            hop(s).start()
+
+        return c
+
+    def serve(d, c):
+        for step in (take, work, close):
+            lax.fori_loop(2 * d, 2 * d + 2, step, 0)
+        return c
+
+    experts(grp)
+    lax.fori_loop(0, 1, serve, 0)
+
+    ent[...] = jnp.zeros(ent.shape, F32)
+    row1 = jnp.zeros((1, hd), F32)
+
+    def enter(g, carry):
+        total, peak, nor = carry
+        for copy in group_arrivals(g):
+            copy.wait_recv()
+        total, peak, mem, nor = join((total, peak, ent[...], nor), unpack(cgrp[g], sgrp[g]))
+        ent[...] = mem
+        return total, peak, nor
+
+    total, peak, nor = lax.fori_loop(0, grp, enter, (row1, row1 + FLOOR, row1))
+    joined = join((total, peak, ent[...], nor), unpack(cpair[0], spair[0]))
+    odd = par == 1
+    m_in = jnp.where(odd, joined[1], peak)
+    n_in = jnp.where(odd, joined[3], nor)
+    c_in = jnp.where(odd, joined[2], ent[...])
+
+    carried = b_col + m_in[:, 0:1]
+    decay = jnp.where(cid <= rid, b_col - b_row + i_row, -jnp.inf)
+    peaks = jnp.maximum(carried, jnp.max(decay, axis=-1, keepdims=True))
+    across = jnp.exp(carried - peaks)
+    scores = dot(q_ref[...], k_ref[...], ((1,), (1,))) * (hd**-0.5) * jnp.exp(decay - peaks)
+    qf = q_ref[...].astype(F32)
+    den = jnp.sum(scores, axis=-1, keepdims=True) + across * jnp.sum(qf * n_in, axis=-1, keepdims=True)
+    num = dot(scores.astype(BF16), v_ref[...]) + across * dot(q_ref[...], c_in.astype(BF16))
+    cell = num / jnp.maximum(jnp.abs(den), jnp.exp(-peaks))
+    head[...] = (cell * hs_ref[...]).astype(BF16)
+
+    def part_copy(j):
+        return pltpu.make_async_remote_copy(
+            src_ref=pout.at[j], dst_ref=prec.at[tp], send_sem=p_ss.at[j], recv_sem=p_rs.at[tp],
+            device_id=(me, j), device_id_type=MESH)
+
+    def part_arrival(j):
+        return pltpu.make_async_remote_copy(
+            src_ref=pout.at[j], dst_ref=prec.at[j], send_sem=p_ss.at[j], recv_sem=p_rs.at[j],
+            device_id=(me, j), device_id_type=MESH)
+
+    def project(j):
+        pout[j] = dot(head[pl.ds(pl.multiple_of(j * rows, rows), rows), :], wo[...]).astype(BF16)
+
+    def send_part(i, c):
+        j = lax.rem(tp + i, nt)
+        project(j)
+        part_copy(j).start()
+        return c
+
+    lax.fori_loop(1, nt, send_part, 0)
+    project(tp)
+
+    lax.fori_loop(1, groups - 1, serve, 0)
+
+    def give_back(j, c):
+        s, valid = where_is(2 * (groups - 1) - 1 - j)
+
+        @pl.when(valid & jnp.logical_not(at_end(s)))
+        def _():
+            mine = combined(s)
+            ret_copy(s, s, grp).wait_recv()
+            part[s] = (mine + ret[s].astype(F32)).astype(BF16)
+            hop(s).start()
+
+        return c
+
+    lax.fori_loop(0, 2 * (groups - 1), give_back, 0)
+
+    def mix(i, total):
+        j = lax.rem(tp + i, nt)
+        part_arrival(j).wait_recv()
+        return total + prec[j].astype(F32)
+
+    projected = pout[tp].astype(F32)
+    for i in range(1, nt):
+        projected = mix(i, projected)
+    mixed_ref[...] = rms(projected, ps_ref[...]).astype(BF16)
+
+    acc[...] = combined(grp)
+    for slot, there in ((grp, grp + 1 < groups), (groups, grp > 0)):
+        @pl.when(there)
+        def _():
+            ret_copy(grp, slot, grp).wait_recv()
+            acc[...] += ret[slot].astype(F32)
+
+    routed_ref[...] = acc[...].astype(BF16)
+
+    def finish(s, c):
+        swap_copy(0, s).wait_send()
+        swap_copy(1, s).wait_send()
+
+        @pl.when(s != grp)
+        def _():
+            hop(s).wait_send()
+            info_copy(s, grp).wait_send()
+
+        for h in range(2):
+            @pl.when((s != grp) & jnp.logical_not(at_end(s)))
+            def _():
+                tok_copy(s, h, grp, s).wait_send()
+
+        return c
+
+    lax.fori_loop(0, groups, finish, 0)
+    for h in range(2):
+        @pl.when(grp + 1 < groups)
+        def _():
+            tok_copy(grp, h, grp, grp).wait_send()
+
+        @pl.when(grp > 0)
+        def _():
+            tok_copy(grp, h, grp, groups).wait_send()
 
     def finish_group(g, c):
         for copy in group_copies(g):
@@ -349,8 +764,31 @@
     hbm = pl.BlockSpec(memory_space=pl.ANY)
     dma = pltpu.SemaphoreType.DMA
     slots = pltpu.VMEM((n, cap, width), BF16)
+    groups = n // 2
+    relay = groups * tokens * width * 6 < 24 * 1024 * 1024
+    wide = -(-tokens // 128) * 128
+    some = pltpu.VMEM((groups, cap, width), BF16)
+    if relay:
+        body = relay_kernel
+        buffers = [
+            pltpu.VMEM((groups, tokens, width), BF16),
+            pltpu.VMEM((groups, 8, wide), F32),
+            some, some, some, some, some,
+            pltpu.VMEM((groups, tokens, width), BF16),
+            pltpu.VMEM((groups + 1, tokens, width), BF16),
+            pltpu.VMEM((tokens, width), F32),
+        ]
+        sems = [dma((groups + 1, 2)), dma((groups, 2))] + [dma((groups,))] * 7 + [dma((groups + 1,))]
+    else:
+        body = kernel
+        buffers = [
+            slots, slots, slots, slots,
+            pltpu.VMEM((tokens, width), BF16),
+            pltpu.VMEM((tokens, width), F32),
+        ]
+        sems = [dma((n,))] * 4
     return pl.pallas_call(
-        functools.partial(kernel, n, nt, cap),
+        functools.partial(body, n, nt, cap),
         out_shape=(
             jax.ShapeDtypeStruct((rows, width), BF16),
             jax.ShapeDtypeStruct((tokens, width), BF16),
@@ -362,9 +800,7 @@
             pltpu.VMEM((width, hidden), BF16),
             pltpu.VMEM((hidden, width), BF16),
             pltpu.VMEM((hd, width), BF16),
-            slots, slots, slots, slots,
-            pltpu.VMEM((tokens, width), BF16),
-            pltpu.VMEM((tokens, width), F32),
+            *buffers,
             pltpu.VMEM((2, hd, hd), BF16),
             pltpu.VMEM((2, 8, hd), F32),
             pltpu.VMEM((n // 2, hd, hd), BF16),
@@ -374,7 +810,7 @@
             pltpu.VMEM((nt, rows, width), BF16),
             pltpu.VMEM((nt, rows, width), BF16),
             dma((4,)),
-            dma((n,)), dma((n,)), dma((n,)), dma((n,)),
+            *sems,
             dma, dma, dma, dma,
             dma((n // 2,)), dma((n // 2,)), dma((n // 2,)), dma((n // 2,)),
             dma((nt,)), dma((nt,)),

time: 169 us -> 151 us (0.89)
  the two profiles are of different devices: /device:TPU:16 before, /device:TPU:0 now
where the time goes in v2:
time: 151 us; the launch traced here: 150 us
  Pallas kernels  141 us (93%)
  local copies, waits for them, and re-layouts  8.3 us (5%)
    pallas_call x1, Pallas kernels, shards(): pl.pallas_call(functools.partial(body, n, nt, cap), out_shape=(jax.ShapeD...  141 us
    unnamed x4, local copies, waits for them, and re-layouts  6.86 us

profile of v2, /device:TPU:0, one launch (start us, length us, event | category | flops | bytes accessed | tf_op | source)
XLA Modules:
  0.0 150.3 jit_solution(3609801528914307580)
XLA Ops:
  0.6 1.4 copy.21.ids_ref
  2.1 1.4 copy.22.grp_ref
  3.5 1.4 copy.23.sc_ref
  5.0 141.3 %shard_map.176 = (bf16[128,2048]{1,0:T(8,128)(2,1)}, bf16[192,2048]{1,0:T(8,128)(2,1)}) custom-call(bf16[512,256]{1,0:T(8,128)(2,1)} %q_ref.1, bf16[512,256]{1,0:T(8,128)(2,1)} %k_ref.1, bf16[512,256]{1,0:T(8,128)(2,1)} %v_ref.1, f32[1,512]{1,0:T(1,128)} %ig_ref.1, f32[1,512]{1,0:T(1,128)} %fg_ref.1, f32[1,512]{1,0:T(1,128)} %fb_ref.1, f32[1,256]{1,0:T(1,128)} %bitcast.7, ...), custom_call_target="tpu_custom_call" | custom-call | tf_op jit(solution)/shard_map/pallas_call | solution.py:790
  146.3 1.9 %copy.26 = bf16[128,2048]{1,0:T(8,128)(2,1)} copy(bf16[128,2048]{1,0:T(8,128)(2,1)} %get-tuple-element.4) | data formatting | bytes 1048576
  148.2 2.1 %copy.27 = bf16[192,2048]{1,0:T(8,128)(2,1)} copy(bf16[192,2048]{1,0:T(8,128)(2,1)} %get-tuple-element.5) | data formatting | bytes 1572864
